TPU v7x, 32 devices: a whole 2x2x4 slice. The times are simulated.
32 devices in a mesh: kv: 4 (over y, x), tp: 8 (over z, core).
Axes of the slice: x: 2, y: 2, z: 4, core: 2. Of those that a mesh axis runs over, the one named last changes fastest.
Arguments:
- tokens: bfloat16 [128, 4096], P(None, 'tp'), may hold values from -6 to 6
- norm_gain: float32 [4096], P('tp'), may hold values from 0.1 to 1.9
- query_weight: bfloat16 [4096, 2048], P('tp', 'kv'), may hold values from -0.09375 to 0.09375
- key_weight: bfloat16 [4096, 2048], P('tp', 'kv'), may hold values from -0.09375 to 0.09375
- value_weight: bfloat16 [4096, 2048], P('tp', 'kv'), may hold values from -0.09375 to 0.09375
- input_gate_weight: bfloat16 [4096, 16], P('tp'), may hold values from -0.09375 to 0.09375
- forget_gate_weight: bfloat16 [4096, 16], P('tp'), may hold values from -0.09375 to 0.09375
- input_gate_bias: float32 [16], P('kv'), may hold values from -2 to 2
- forget_gate_bias: float32 [16], P('kv'), may hold values from 1 to 6
- memory_state: float32 [128, 16, 128, 128], P('tp', 'kv'), may hold values from -12 to 12
- normalizer_state: float32 [128, 16, 128], P('tp', 'kv'), may hold values from -24 to 24
- stabilizer_state: float32 [128, 16], P('tp', 'kv'), may hold values from -1 to 3
- block_keys: bfloat16 [128, 16, 128, 128], P('tp', 'kv'), may hold values from -6 to 6
- block_values: bfloat16 [128, 16, 128, 128], P('tp', 'kv'), may hold values from -6 to 6
- block_input_pre: float32 [128, 16, 128], P('tp', 'kv'), may hold values from -6 to 6
- block_forget_pre: float32 [128, 16, 128], P('tp', 'kv'), may hold values from -6 to 6
- block_lengths: int32 [128], P('tp'), may hold values from 1 to 128, 6553 in all
- head_norm_gain: float32 [2048], P('kv'), may hold values from 0.1 to 1.9
- output_weight: bfloat16 [2048, 4096], P('kv', 'tp'), may hold values from -0.125 to 0.125
- mixer_norm_gain: float32 [4096], P('tp'), may hold values from 0.1 to 1.9
- gate_weight: bfloat16 [4096, 11264], P('tp', 'kv'), may hold values from -0.09375 to 0.09375
- up_weight: bfloat16 [4096, 11264], P('tp', 'kv'), may hold values from -0.09375 to 0.09375
- down_weight: bfloat16 [11264, 4096], P('kv', 'tp'), may hold values from -0.0546875 to 0.0546875
Outputs:
- layer_output: float32 [128, 4096], P(None, 'tp')
Inputs may be any that keep to these rules, and one draw needn't show every extreme that they name: `block_lengths`: some sequence has exactly 128 live positions.
All inputs are finite; a program needn't handle non-finite values. No bound on the sum of `block_lengths` on one device may be relied on, other than what follows from the above.
Results may differ from a plain program's by a relative error of at most 0.0078.
Values may be sent and summed in bfloat16 or wider, within the bound.
No kernel may reach another device: no remote copies, remote signals or barrier semaphores. Data moves between devices by JAX's collectives and lax.ppermute only.
A program may use at most 64 MiB of HBM per device.

v0:
```python
import jax
import jax.numpy as jnp
from jax import lax
from jax.sharding import PartitionSpec as P

D = 4096
epsilon = 1e-06


def memory_cell(
    queries,
    new_keys,
    new_values,
    log_input,
    log_forget,
    memory,
    normalizer,
    stabilizer,
    cached_keys,
    cached_values,
    input_pre,
    forget_pre,
    lengths,
    input_bias,
    forget_bias,
):
    positions = jnp.arange(cached_keys.shape[2])
    is_live = (positions[None, :] < lengths[:, None])[:, None, :]
    cached_input = input_pre + input_bias[None, :, None]
    cached_forget = jnp.where(
        is_live, jax.nn.log_sigmoid(forget_pre + forget_bias[None, :, None]), 0.0
    )
    after_mask = (positions[:, None] > positions[None, :]).astype(jnp.float32)
    later_forget = (
        jnp.einsum("bhu,us->bhs", cached_forget, after_mask, precision=lax.Precision.HIGHEST)
        + log_forget[..., None]
    )
    total_forget = jnp.sum(cached_forget, axis=-1) + log_forget
    exponent = jnp.where(is_live, later_forget + cached_input, -jnp.inf)
    carried = total_forget + stabilizer
    stab_max = jnp.maximum(jnp.maximum(jnp.max(exponent, axis=-1), carried), log_input)
    scores = jnp.einsum("bhd,bhsd->bhs", queries, cached_keys, preferred_element_type=jnp.float32)
    block_weight = jnp.exp(exponent - stab_max[..., None]) * scores
    block_probs = block_weight.astype(jnp.bfloat16)
    block_sum = jnp.einsum(
        "bhs,bhsd->bhd", block_probs, cached_values, preferred_element_type=jnp.float32
    )
    query_wide = queries.astype(jnp.float32)
    new_weight = jnp.exp(log_input - stab_max) * jnp.sum(
        query_wide * new_keys.astype(jnp.float32), axis=-1
    )
    state_weight = jnp.exp(carried - stab_max)
    state_sum = jnp.einsum("bhkv,bhk->bhv", memory, query_wide, precision=lax.Precision.HIGHEST)
    state_norm = jnp.sum(normalizer * query_wide, axis=-1)
    numerator = (
        block_sum
        + new_weight[..., None] * new_values.astype(jnp.float32)
        + state_weight[..., None] * state_sum
    )
    denominator = jnp.sum(block_weight, axis=-1) + new_weight + state_weight * state_norm
    return numerator / jnp.maximum(jnp.abs(denominator), 1.0)[..., None]


def head_scale(cell_out, gain):
    return (cell_out * gain.reshape(cell_out.shape[1], cell_out.shape[2])).astype(jnp.bfloat16)


def activate(gate_sum, up_sum, square_sum):
    row_scale = lax.rsqrt(square_sum / D + epsilon)[:, None]
    return (jax.nn.silu(gate_sum * row_scale) * (up_sum * row_scale)).astype(jnp.bfloat16)


def body(
    tokens,
    norm_gain,
    query_weight,
    key_weight,
    value_weight,
    input_gate_weight,
    forget_gate_weight,
    input_gate_bias,
    forget_gate_bias,
    memory_state,
    normalizer_state,
    stabilizer_state,
    block_keys,
    block_values,
    block_input_pre,
    block_forget_pre,
    block_lengths,
    head_norm_gain,
    output_weight,
    mixer_norm_gain,
    gate_weight,
    up_weight,
    down_weight,
):
    seq_rows = block_keys.shape[0]
    heads_dev = block_keys.shape[1]
    head_size = block_keys.shape[3]
    tok_wide = tokens.astype(jnp.float32)
    scaled_in = (tok_wide * norm_gain).astype(jnp.bfloat16)
    square_part = jnp.sum(tok_wide * tok_wide, axis=1)

    def partial_of(weight):
        return jnp.dot(scaled_in, weight, preferred_element_type=jnp.float32)

    query_sum, key_sum, value_sum, input_sum, forget_sum, square_sum = (
        lax.psum_scatter(partial_of(query_weight), "tp", scatter_dimension=0, tiled=True),
        lax.psum_scatter(partial_of(key_weight), "tp", scatter_dimension=0, tiled=True),
        lax.psum_scatter(partial_of(value_weight), "tp", scatter_dimension=0, tiled=True),
        lax.psum_scatter(partial_of(input_gate_weight), "tp", scatter_dimension=0, tiled=True),
        lax.psum_scatter(partial_of(forget_gate_weight), "tp", scatter_dimension=0, tiled=True),
        lax.psum_scatter(square_part, "tp", scatter_dimension=0, tiled=True),
    )
    first_scale = lax.rsqrt(square_sum / D + epsilon)[:, None]
    queries = (
        (query_sum * first_scale * head_size ** (-0.5))
        .astype(jnp.bfloat16)
        .reshape(seq_rows, heads_dev, head_size)
    )
    new_keys = (key_sum * first_scale).astype(jnp.bfloat16).reshape(seq_rows, heads_dev, head_size)
    new_values = (
        (value_sum * first_scale).astype(jnp.bfloat16).reshape(seq_rows, heads_dev, head_size)
    )
    head_start = lax.axis_index("kv") * heads_dev
    log_input = (
        lax.dynamic_slice_in_dim(input_sum * first_scale, head_start, heads_dev, 1)
        + input_gate_bias
    )
    log_forget = jax.nn.log_sigmoid(
        lax.dynamic_slice_in_dim(forget_sum * first_scale, head_start, heads_dev, 1)
        + forget_gate_bias
    )
    cell_out = memory_cell(
        queries,
        new_keys,
        new_values,
        log_input,
        log_forget,
        memory_state,
        normalizer_state,
        stabilizer_state,
        block_keys,
        block_values,
        block_input_pre,
        block_forget_pre,
        block_lengths,
        input_gate_bias,
        forget_gate_bias,
    )
    head_out = head_scale(cell_out, head_norm_gain).reshape(seq_rows, heads_dev * head_size)
    attended_part = jnp.dot(
        lax.all_gather(head_out, "tp", axis=0, tiled=True),
        output_weight,
        preferred_element_type=jnp.float32,
    )
    attended = lax.psum(attended_part, "kv")
    res_wide = tok_wide + attended
    mid_square = jnp.sum(res_wide * res_wide, axis=1)
    mid_scaled = (res_wide * mixer_norm_gain).astype(jnp.bfloat16)
    gate_part = jnp.dot(mid_scaled, gate_weight, preferred_element_type=jnp.float32)
    up_part = jnp.dot(mid_scaled, up_weight, preferred_element_type=jnp.float32)
    gate_sum, up_sum, mid_sum = lax.psum((gate_part, up_part, mid_square), "tp")
    hidden = activate(gate_sum, up_sum, mid_sum)
    down_part = jnp.dot(hidden, down_weight, preferred_element_type=jnp.float32)
    mixed = lax.psum(down_part, "kv")
    return res_wide + mixed


def solution(mesh):
    placed = (
        P(None, "tp"),
        P("tp"),
        P("tp", "kv"),
        P("tp", "kv"),
        P("tp", "kv"),
        P("tp", None),
        P("tp", None),
        P("kv"),
        P("kv"),
        P("tp", "kv", None, None),
        P("tp", "kv", None),
        P("tp", "kv"),
        P("tp", "kv", None, None),
        P("tp", "kv", None, None),
        P("tp", "kv", None),
        P("tp", "kv", None),
        P("tp"),
        P("kv"),
        P("kv", "tp"),
        P("tp"),
        P("tp", "kv"),
        P("tp", "kv"),
        P("kv", "tp"),
    )
    return jax.shard_map(body, mesh=mesh, in_specs=placed, out_specs=P(None, "tp"), check_vma=False)
```

profile of v0, /device:TPU:0, one launch (start us, length us, event | category | flops | bytes accessed | tf_op | source)
XLA Modules:
  0.0 376.3 jit_solution(17206025061885807073)
XLA Ops:
  6.6 1.9 fusion.16
  8.5 1.7 fusion.14
  10.3 2.1 fusion.12
  12.5 2.1 fusion.10
  14.6 0.9 fusion.8
  15.8 18.1 %all-reduce = f32[128]{0:T(128)S(1)} all-reduce(f32[128]{0:T(128)S(1)} %fusion.4), channel_id=3, replica_groups=mesh['kv'=4,'tp'=8] {'tp'}, use_global_device_ids=true, to_apply=%region_2.0.clone | all-reduce | flops 128 | bytes 1024
  34.6 1.3 dynamic-slice
  36.7 0.9 fusion.32
  37.7 5.3 %reduce-scatter.16.cloned.1.call-done = f32[16,16]{1,0:T(8,128)} async-done(((f32[128,16]{1,0:T(8,128)}), f32[16,16]{1,0:T(8,128)}) %reduce-scatter.16.cloned.1.call-update) | async-done | bytes 1040
  43.9 29.9 %reduce-scatter.18.cloned.1.call-done = f32[16,16]{1,0:T(8,128)} async-done(((f32[128,16]{1,0:T(8,128)}), f32[16,16]{1,0:T(8,128)}) %reduce-scatter.18.cloned.1.call-update) | async-done | bytes 1040
  74.6 1.6 fusion.34
  76.9 27.9 %reduce-scatter.10.cloned.1.call-done = f32[16,512]{1,0:T(8,128)} async-done(((f32[128,512]{1,0:T(8,128)}), f32[16,512]{1,0:T(8,128)}) %reduce-scatter.10.cloned.1.call-update) | async-done | bytes 32784 | tf_op jit(solution)/shard_map/reduce_scatter | solution.py:109
  104.9 31.1 %reduce-scatter.12.cloned.1.call-done = f32[16,512]{1,0:T(8,128)} async-done(((f32[128,512]{1,0:T(8,128)}), f32[16,512]{1,0:T(8,128)}) %reduce-scatter.12.cloned.1.call-update) | async-done | bytes 32784 | tf_op jit(solution)/shard_map/reduce_scatter | solution.py:110
  136.0 31.1 %reduce-scatter.14.cloned.1.call-done = f32[16,512]{1,0:T(8,128)} async-done(((f32[128,512]{1,0:T(8,128)}), f32[16,512]{1,0:T(8,128)}) %reduce-scatter.14.cloned.1.call-update) | async-done | bytes 32784 | tf_op jit(solution)/shard_map/reduce_scatter | solution.py:111
  167.0 1.5 fusion.25
  170.8 4.9 %fusion.36 = f32[16,4,1,128]{3,2,1,0:T(1,128)} fusion(bf16[16,4,128,1]{2,3,1,0:T(2,128)(2,1)S(1)} %reshape.54, f32[16,4,128,128]{3,2,1,0:T(8,128)} %param.32), kind=kOutput, calls=%fused_computation.61 | convolution fusion | flops 12582912 | bytes 4243456 | tf_op jit(solution)/shard_map/bhkv,bhk->bhv/dot_general | solution.py:53
  175.8 2.0 fusion.35
  178.8 1.3 copy.52
  180.1 1.3 copy.49
  181.5 1.3 copy.50
  182.8 1.4 reshape.46
  184.2 2.3 fusion.22
  186.7 14.0 %all_gather.3 = bf16[128,512]{1,0:T(8,128)(2,1)S(1)} all-gather(bf16[16,512]{1,0:T(8,128)(2,1)S(1)} %bitcast.45), channel_id=1, replica_groups=mesh['kv'=4,'tp'=8] {'tp'}, dimensions={0}, use_global_device_ids=true | all-gather | bytes 147456 | tf_op jit(solution)/shard_map/all_gather | solution.py:154
  201.7 41.3 %all-reduce.6.cloned.1.call-done = f32[128,512]{1,0:T(8,128)} async-done(((f32[128,512]{1,0:T(8,128)}), f32[128,512]{1,0:T(8,128)}) %all-reduce.6.cloned.1.call-update) | async-done | bytes 262160 | tf_op jit(solution)/shard_map/psum | solution.py:158
  243.0 1.1 multiply_reduce_fusion
  244.1 1.7 fusion.39
  246.4 1.7 fusion.38
  248.2 16.2 %psum.37 = f32[128]{0:T(128)S(1)} all-reduce(f32[128]{0:T(128)S(1)} %get-tuple-element.12), channel_id=1, replica_groups=mesh['kv'=4,'tp'=8] {'tp'}, use_global_device_ids=true, to_apply=%region_15.16 | all-reduce | flops 128 | bytes 1024 | tf_op jit(solution)/shard_map/psum | solution.py:164
  264.4 56.5 %all-reduce.10.cloned.1.call-done = (f32[128,2816]{1,0:T(8,128)}, f32[128,2816]{1,0:T(8,128)}) async-done(((f32[128,2816]{1,0:T(8,128)}, f32[128,2816]{1,0:T(8,128)}), (f32[128,2816]{1,0:T(8,128)}, f32[128,2816]{1,0:T(8,128)})) %all-reduce.10.cloned.1.call-update) | async-done | bytes 2883600 | tf_op jit(solution)/shard_map/psum | solution.py:164
  320.9 4.2 %fusion.2 = f32[128,512]{1,0:T(8,128)} fusion(bf16[2816,512]{1,0:T(8,128)(2,1)} %param.45, f32[128,2816]{1,0:T(8,128)} %get-tuple-element.7, f32[128,2816]{1,0:T(8,128)} %get-tuple-element.8, f32[128]{0:T(128)S(1)} %add_rsqrt_fusion), kind=kOutput, calls=%fused_computation.4 | convolution fusion | flops 371982336 | bytes 6029824 | tf_op jit(solution)/shard_map/dot_general | solution.py:166
  325.1 42.7 %all-reduce.8.cloned.1.call-done = f32[128,512]{1,0:T(8,128)} async-done(((f32[128,512]{1,0:T(8,128)}), f32[128,512]{1,0:T(8,128)}) %all-reduce.8.cloned.1.call-update) | async-done | bytes 262160 | tf_op jit(solution)/shard_map/psum | solution.py:167
  367.8 1.7 fusion.5
  (103 shorter events, 8.8 us)
Async XLA Ops:
  6.5 237.5 %copy-start = (bf16[512,2816]{1,0:T(8,128)(2,1)S(1)}, bf16[512,2816]{1,0:T(8,128)(2,1)}, u32[]{:S(2)}) copy-start(bf16[512,2816]{1,0:T(8,128)(2,1)} %param.44) | copy-start | bytes 8650756
  6.5 8.1 %copy-start.1 = (bf16[128,512]{1,0:T(8,128)(2,1)S(1)}, bf16[128,512]{1,0:T(8,128)(2,1)}, u32[]{:S(2)}) copy-start(bf16[128,512]{1,0:T(8,128)(2,1)} %param.23) | copy-start | bytes 393220
  6.5 8.1 %copy-start.10 = (f32[512]{0:T(512)S(1)}, f32[512]{0:T(512)}, u32[]{:S(2)}) copy-start(f32[512]{0:T(512)} %param.24) | copy-start | bytes 6148
  6.5 8.1 %copy-start.5 = (bf16[512,512]{1,0:T(8,128)(2,1)S(1)}, bf16[512,512]{1,0:T(8,128)(2,1)}, u32[]{:S(2)}) copy-start(bf16[512,512]{1,0:T(8,128)(2,1)} %param.27) | copy-start | bytes 1572868
  6.5 36.4 %reduce-scatter.16.cloned.1.call-start = ((), (), s32[]{:S(2)}) async-start(), calls=%async_computation.10 | async-start | bytes 73728
  8.5 28.2 %copy-start.22 = (f32[4]{0:T(128)S(1)}, f32[4]{0:T(128)}, u32[]{:S(2)}) copy-start(f32[4]{0:T(128)} %param.31) | copy-start | bytes 52
  8.5 66.2 %copy-start.31 = (f32[4]{0:T(128)S(1)}, f32[4]{0:T(128)}, u32[]{:S(2)}) copy-start(f32[4]{0:T(128)} %param.30) | copy-start | bytes 52
  8.5 65.3 %reduce-scatter.18.cloned.1.call-start = ((), (), s32[]{:S(2)}) async-start(), calls=%async_computation.11 | async-start | bytes 73728
  10.2 66.0 %copy-start.26 = (f32[16,4]{0,1:T(4,128)S(1)}, f32[16,4]{0,1:T(4,128)}, u32[]{:S(2)}) copy-start(f32[16,4]{0,1:T(4,128)} %param.34) | copy-start | bytes 772
  10.3 94.6 %reduce-scatter.10.cloned.1.call-start = ((), (), s32[]{:S(2)}) async-start(), calls=%async_computation.5 | async-start | bytes 294912 | tf_op jit(solution)/shard_map/reduce_scatter | solution.py:109
  12.4 123.5 %reduce-scatter.12.cloned.1.call-start = ((), (), s32[]{:S(2)}) async-start(), calls=%async_computation.6 | async-start | bytes 294912 | tf_op jit(solution)/shard_map/reduce_scatter | solution.py:110
  14.6 152.5 %reduce-scatter.14.cloned.1.call-start = ((), (), s32[]{:S(2)}) async-start(), calls=%async_computation.7 | async-start | bytes 294912 | tf_op jit(solution)/shard_map/reduce_scatter | solution.py:111
  15.6 227.4 %all-reduce.6.cloned.1.call-start = ((), (), s32[]{:S(2)}) async-start(), calls=%async_computation.8 | async-start | bytes 524288 | tf_op jit(solution)/shard_map/psum | solution.py:158
  36.7 131.8 %copy-start.24 = (f32[16]{0:T(128)}, f32[16]{0:T(128)S(1)}, u32[]{:S(2)}) copy-start(f32[16]{0:T(128)S(1)} %fusion.30) | copy-start | bytes 196
  37.6 130.9 %copy-start.17 = (f32[16,4]{0,1:T(4,128)}, f32[16,4]{0,1:T(4,128)S(1)}, u32[]{:S(2)}) copy-start(f32[16,4]{0,1:T(4,128)S(1)} %fusion.32) | copy-start | bytes 772
  43.8 124.7 %copy-start.14 = (f32[16,4]{0,1:T(4,128)}, f32[16,4]{0,1:T(4,128)S(1)}, u32[]{:S(2)}) copy-start(f32[16,4]{0,1:T(4,128)S(1)} %copy.64) | copy-start | bytes 772
  74.6 93.9 %copy-start.19 = (f32[16,4]{0,1:T(4,128)}, f32[16,4]{0,1:T(4,128)S(1)}, u32[]{:S(2)}) copy-start(f32[16,4]{0,1:T(4,128)S(1)} %copy.65) | copy-start | bytes 772
  170.8 4.9 %copy-start.3 = (bf16[16,4,128,128]{3,2,1,0:T(8,128)(2,1)S(1)}, bf16[16,4,128,128]{3,2,1,0:T(8,128)(2,1)}, u32[]{:S(2)}) copy-start(bf16[16,4,128,128]{3,2,1,0:T(8,128)(2,1)} %param.35) | copy-start | bytes 6291460
  175.7 2.3 copy-start.15
  175.7 2.3 copy-start.18
  175.7 2.3 copy-start.20
  175.8 24.9 %copy-start.6 = (bf16[512,512]{1,0:T(8,128)(2,1)S(1)}, bf16[512,512]{1,0:T(8,128)(2,1)}, u32[]{:S(2)}) copy-start(bf16[512,512]{1,0:T(8,128)(2,1)} %param.41) | copy-start | bytes 1572868
  184.2 2.3 copy-start.8
  184.2 2.3 copy-start.9
  184.2 2.3 copy-start.11
  184.2 2.3 copy-start.12
  184.2 2.3 copy-start.13
  184.2 2.3 copy-start.30
  201.6 119.3 %all-reduce.10.cloned.1.call-start = ((), (), s32[]{:S(2)}) async-start(), calls=%async_computation.12 | async-start | bytes 5767168 | tf_op jit(solution)/shard_map/psum | solution.py:164
  244.0 2.3 copy-start.2
  248.1 119.7 %all-reduce.8.cloned.1.call-start = ((), (), s32[]{:S(2)}) async-start(), calls=%async_computation.9 | async-start | bytes 524288 | tf_op jit(solution)/shard_map/psum | solution.py:167
  320.9 46.9 %copy-start.4 = (f32[128,512]{1,0:T(8,128)S(1)}, f32[128,512]{1,0:T(8,128)}, u32[]{:S(2)}) copy-start(f32[128,512]{1,0:T(8,128)} %all-reduce.6.cloned.1.call-done) | copy-start | bytes 786436
  (9 other events, 20.1 us)
Sparse Core Ops, SparseCore 0:
  9.6 33.3 reduce-scatter.15
  45.2 28.5 reduce-scatter.17
  76.0 28.8 reduce-scatter.9
  107.0 28.9 reduce-scatter.11
  138.0 28.9 reduce-scatter.13
  201.8 41.1 all-reduce.5
  248.2 72.6 all-reduce.9
  325.2 42.5 all-reduce.7
where the time goes:
time: 377 us; the launch traced here: 376 us
  waiting for transfers between devices  266 us (71%)
  blocking collectives  48.3 us (13%)
  matrix products  28 us (7%)
  between operations  14.5 us (4%)
  local copies, waits for them, and re-layouts  10.6 us (3%)
  other arithmetic  8.77 us (2%)
    psum x1, waiting for transfers between devices, body(): gate_sum, up_sum, mid_sum = lax.psum((gate_part, up_part, mid_square), 'tp')  56.5 us
    psum x1, waiting for transfers between devices, body(): mixed = lax.psum(down_part, 'kv')  42.7 us
    psum x1, waiting for transfers between devices, body(): attended = lax.psum(attended_part, 'kv')  41.3 us
    unnamed x10, waiting for transfers between devices  35.3 us
    reduce_scatter x1, waiting for transfers between devices, body(): lax.psum_scatter(partial_of(key_weight), 'tp', scatter_dimension=0, tiled...  31.1 us
    reduce_scatter x1, waiting for transfers between devices, body(): lax.psum_scatter(partial_of(value_weight), 'tp', scatter_dimension=0, til...  31.1 us
    reduce_scatter x1, waiting for transfers between devices, body(): lax.psum_scatter(partial_of(query_weight), 'tp', scatter_dimension=0, til...  27.9 us
    unnamed x1, blocking collectives  18.1 us
  transfers between devices with their start and end apart: 8, of which 8 were waited for; matrix products, arithmetic and copies ran while one was open for 4% of the time, Pallas kernels for 0%

commit v1 on v0

--- a/solution.py
+++ b/solution.py
@@ -164,7 +164,9 @@
     gate_sum, up_sum, mid_sum = lax.psum((gate_part, up_part, mid_square), "tp")
     hidden = activate(gate_sum, up_sum, mid_sum)
     down_part = jnp.dot(hidden, down_weight, preferred_element_type=jnp.float32)
-    mixed = lax.psum(down_part, "kv")
+    mixed = down_part
+    for hop in (1, 2):
+        mixed = mixed + lax.ppermute(mixed, "kv", [(dev, dev ^ hop) for dev in range(4)])
     return res_wide + mixed
 
 

time: 377 us -> 346 us (0.918)
  waiting for transfers between devices: 266 us -> 234 us
    psum x1 -> x0, waiting for transfers between devices: 42.7 us -> none  [body(): mixed = lax.psum(down_part, 'kv')]
    ppermute x0 -> x2, waiting for transfers between devices: none -> 10.4 us  [body(): lax.ppermute(mixed, 'kv', [(dev, dev ^ hop) for dev in range(4)])]
    unnamed x10 -> x9, waiting for transfers between devices: 35.3 us -> 35.5 us
  transfers between devices with their start and end apart: 8 -> 9, of which waited for: 8 -> 9; matrix products, arithmetic and copies ran while one was open for 4% -> 4% of each run, Pallas kernels for 0% -> 0%
where the time goes in v1:
time: 346 us
  waiting for transfers between devices  234 us (68%)
  blocking collectives  48.4 us (14%)
  matrix products  27.2 us (8%)
  between operations  14.4 us (4%)
  local copies, waits for them, and re-layouts  10.5 us (3%)
  other arithmetic  7.87 us (2%)
    psum x1, waiting for transfers between devices, body(): gate_sum, up_sum, mid_sum = lax.psum((gate_part, up_part, mid_square), 'tp')  56.5 us
    psum x1, waiting for transfers between devices, body(): attended = lax.psum(attended_part, 'kv')  41.3 us
    unnamed x9, waiting for transfers between devices  35.5 us
    reduce_scatter x1, waiting for transfers between devices, body(): lax.psum_scatter(partial_of(value_weight), 'tp', scatter_dimension=0, til...  31.1 us
    reduce_scatter x1, waiting for transfers between devices, body(): lax.psum_scatter(partial_of(key_weight), 'tp', scatter_dimension=0, tiled...  31 us
    reduce_scatter x1, waiting for transfers between devices, body(): lax.psum_scatter(partial_of(query_weight), 'tp', scatter_dimension=0, til...  28 us
    unnamed x1, blocking collectives  18.1 us
    psum x1, blocking collectives, body(): gate_sum, up_sum, mid_sum = lax.psum((gate_part, up_part, mid_square), 'tp')  16.3 us
  transfers between devices with their start and end apart: 9, of which 9 were waited for; matrix products, arithmetic and copies ran while one was open for 4% of the time, Pallas kernels for 0%

profile of v1, /device:TPU:0, one launch (start us, length us, event | category | flops | bytes accessed | tf_op | source)
XLA Modules:
  0.0 345.5 jit_solution(9697295924172435305)
XLA Ops:
  6.6 1.9 fusion.15
  8.5 1.7 fusion.13
  10.3 2.1 fusion.11
  12.5 2.1 fusion.9
  15.8 18.1 %all-reduce = f32[128]{0:T(128)S(1)} all-reduce(f32[128]{0:T(128)S(1)} %fusion.4), channel_id=3, replica_groups=mesh['kv'=4,'tp'=8] {'tp'}, use_global_device_ids=true, to_apply=%region_2.0.clone | all-reduce | flops 128 | bytes 1024
  34.6 1.2 dynamic-slice
  37.4 5.5 %reduce-scatter.16.cloned.1.call-done = f32[16,16]{1,0:T(8,128)} async-done(((f32[128,16]{1,0:T(8,128)}), f32[16,16]{1,0:T(8,128)}) %reduce-scatter.16.cloned.1.call-update) | async-done | bytes 1040
  43.9 29.9 %reduce-scatter.18.cloned.1.call-done = f32[16,16]{1,0:T(8,128)} async-done(((f32[128,16]{1,0:T(8,128)}), f32[16,16]{1,0:T(8,128)}) %reduce-scatter.18.cloned.1.call-update) | async-done | bytes 1040
  74.6 1.6 fusion.33
  76.9 28.0 %reduce-scatter.10.cloned.1.call-done = f32[16,512]{1,0:T(8,128)} async-done(((f32[128,512]{1,0:T(8,128)}), f32[16,512]{1,0:T(8,128)}) %reduce-scatter.10.cloned.1.call-update) | async-done | bytes 32784 | tf_op jit(solution)/shard_map/reduce_scatter | solution.py:109
  104.9 31.0 %reduce-scatter.12.cloned.1.call-done = f32[16,512]{1,0:T(8,128)} async-done(((f32[128,512]{1,0:T(8,128)}), f32[16,512]{1,0:T(8,128)}) %reduce-scatter.12.cloned.1.call-update) | async-done | bytes 32784 | tf_op jit(solution)/shard_map/reduce_scatter | solution.py:110
  135.9 31.1 %reduce-scatter.14.cloned.1.call-done = f32[16,512]{1,0:T(8,128)} async-done(((f32[128,512]{1,0:T(8,128)}), f32[16,512]{1,0:T(8,128)}) %reduce-scatter.14.cloned.1.call-update) | async-done | bytes 32784 | tf_op jit(solution)/shard_map/reduce_scatter | solution.py:111
  167.0 1.5 fusion.24
  170.8 4.9 %fusion.35 = f32[16,4,1,128]{3,2,1,0:T(1,128)} fusion(bf16[16,4,128,1]{2,3,1,0:T(2,128)(2,1)S(1)} %reshape.54, f32[16,4,128,128]{3,2,1,0:T(8,128)} %param.32), kind=kOutput, calls=%fused_computation.61 | convolution fusion | flops 12582912 | bytes 4243456 | tf_op jit(solution)/shard_map/bhkv,bhk->bhv/dot_general | solution.py:53
  175.8 2.0 fusion.34
  178.8 1.3 copy.52
  180.1 1.3 copy.49
  181.4 1.4 copy.50
  182.8 1.4 reshape.46
  184.2 2.3 fusion.21
  186.7 14.0 %all_gather.3 = bf16[128,512]{1,0:T(8,128)(2,1)S(1)} all-gather(bf16[16,512]{1,0:T(8,128)(2,1)S(1)} %bitcast.45), channel_id=1, replica_groups=mesh['kv'=4,'tp'=8] {'tp'}, dimensions={0}, use_global_device_ids=true | all-gather | bytes 147456 | tf_op jit(solution)/shard_map/all_gather | solution.py:154
  201.7 41.3 %all-reduce.5.cloned.1.call-done = f32[128,512]{1,0:T(8,128)} async-done(((f32[128,512]{1,0:T(8,128)}), f32[128,512]{1,0:T(8,128)}) %all-reduce.5.cloned.1.call-update) | async-done | bytes 262160 | tf_op jit(solution)/shard_map/psum | solution.py:158
  243.0 1.1 multiply_reduce_fusion
  244.1 1.7 fusion.38
  246.4 1.7 fusion.37
  248.1 16.3 %psum.30 = f32[128]{0:T(128)S(1)} all-reduce(f32[128]{0:T(128)S(1)} %get-tuple-element.12), channel_id=1, replica_groups=mesh['kv'=4,'tp'=8] {'tp'}, use_global_device_ids=true, to_apply=%region_15.16 | all-reduce | flops 128 | bytes 1024 | tf_op jit(solution)/shard_map/psum | solution.py:164
  264.4 56.5 %all-reduce.7.cloned.1.call-done = (f32[128,2816]{1,0:T(8,128)}, f32[128,2816]{1,0:T(8,128)}) async-done(((f32[128,2816]{1,0:T(8,128)}, f32[128,2816]{1,0:T(8,128)}), (f32[128,2816]{1,0:T(8,128)}, f32[128,2816]{1,0:T(8,128)})) %all-reduce.7.cloned.1.call-update) | async-done | bytes 2883600 | tf_op jit(solution)/shard_map/psum | solution.py:164
  320.9 3.4 fusion.2
  324.4 1.5 collective-permute-start
  325.9 5.5 %collective-permute-done = f32[128,512]{1,0:T(8,128)S(1)} collective-permute-done((f32[128,512]{1,0:T(8,128)S(1)}, f32[128,512]{1,0:T(8,128)S(1)}, u32[]{:S(2)}, u32[]{:S(2)}) %collective-permute-start) | collective-permute-done | bytes 262176 | tf_op jit(solution)/shard_map/ppermute | solution.py:169
  331.5 1.5 collective-permute-start.1
  333.0 4.9 %collective-permute-done.1 = f32[128,512]{1,0:T(8,128)S(1)} collective-permute-done((f32[128,512]{1,0:T(8,128)S(1)}, f32[128,512]{1,0:T(8,128)S(1)}, u32[]{:S(2)}, u32[]{:S(2)}) %collective-permute-start.1) | collective-permute-done | bytes 262176 | tf_op jit(solution)/shard_map/ppermute | solution.py:169
  (105 shorter events, 11.4 us)
Async XLA Ops:
  6.5 237.5 %copy-start = (bf16[512,2816]{1,0:T(8,128)(2,1)S(1)}, bf16[512,2816]{1,0:T(8,128)(2,1)}, u32[]{:S(2)}) copy-start(bf16[512,2816]{1,0:T(8,128)(2,1)} %param.44) | copy-start | bytes 8650756
  6.5 8.1 %copy-start.1 = (bf16[128,512]{1,0:T(8,128)(2,1)S(1)}, bf16[128,512]{1,0:T(8,128)(2,1)}, u32[]{:S(2)}) copy-start(bf16[128,512]{1,0:T(8,128)(2,1)} %param.23) | copy-start | bytes 393220
  6.5 8.1 %copy-start.10 = (f32[512]{0:T(512)S(1)}, f32[512]{0:T(512)}, u32[]{:S(2)}) copy-start(f32[512]{0:T(512)} %param.24) | copy-start | bytes 6148
  6.5 8.1 %copy-start.5 = (bf16[512,512]{1,0:T(8,128)(2,1)S(1)}, bf16[512,512]{1,0:T(8,128)(2,1)}, u32[]{:S(2)}) copy-start(bf16[512,512]{1,0:T(8,128)(2,1)} %param.27) | copy-start | bytes 1572868
  6.5 36.4 %reduce-scatter.16.cloned.1.call-start = ((), (), s32[]{:S(2)}) async-start(), calls=%async_computation.9 | async-start | bytes 73728
  8.4 28.0 %copy-start.22 = (f32[4]{0:T(128)S(1)}, f32[4]{0:T(128)}, u32[]{:S(2)}) copy-start(f32[4]{0:T(128)} %param.31) | copy-start | bytes 52
  8.5 66.2 %copy-start.31 = (f32[4]{0:T(128)S(1)}, f32[4]{0:T(128)}, u32[]{:S(2)}) copy-start(f32[4]{0:T(128)} %param.30) | copy-start | bytes 52
  8.5 65.3 %reduce-scatter.18.cloned.1.call-start = ((), (), s32[]{:S(2)}) async-start(), calls=%async_computation.10 | async-start | bytes 73728
  10.2 66.0 %copy-start.26 = (f32[16,4]{0,1:T(4,128)S(1)}, f32[16,4]{0,1:T(4,128)}, u32[]{:S(2)}) copy-start(f32[16,4]{0,1:T(4,128)} %param.34) | copy-start | bytes 772
  10.3 94.6 %reduce-scatter.10.cloned.1.call-start = ((), (), s32[]{:S(2)}) async-start(), calls=%async_computation.5 | async-start | bytes 294912 | tf_op jit(solution)/shard_map/reduce_scatter | solution.py:109
  12.4 123.5 %reduce-scatter.12.cloned.1.call-start = ((), (), s32[]{:S(2)}) async-start(), calls=%async_computation.6 | async-start | bytes 294912 | tf_op jit(solution)/shard_map/reduce_scatter | solution.py:110
  14.5 152.5 %reduce-scatter.14.cloned.1.call-start = ((), (), s32[]{:S(2)}) async-start(), calls=%async_computation.7 | async-start | bytes 294912 | tf_op jit(solution)/shard_map/reduce_scatter | solution.py:111
  15.6 227.4 %all-reduce.5.cloned.1.call-start = ((), (), s32[]{:S(2)}) async-start(), calls=%async_computation.8 | async-start | bytes 524288 | tf_op jit(solution)/shard_map/psum | solution.py:158
  36.5 132.0 %copy-start.24 = (f32[16]{0:T(128)}, f32[16]{0:T(128)S(1)}, u32[]{:S(2)}) copy-start(f32[16]{0:T(128)S(1)} %fusion.29) | copy-start | bytes 196
  37.4 131.1 %copy-start.17 = (f32[16,4]{0,1:T(4,128)}, f32[16,4]{0,1:T(4,128)S(1)}, u32[]{:S(2)}) copy-start(f32[16,4]{0,1:T(4,128)S(1)} %fusion.31) | copy-start | bytes 772
  43.8 124.7 %copy-start.14 = (f32[16,4]{0,1:T(4,128)}, f32[16,4]{0,1:T(4,128)S(1)}, u32[]{:S(2)}) copy-start(f32[16,4]{0,1:T(4,128)S(1)} %copy.64) | copy-start | bytes 772
  74.6 93.9 %copy-start.19 = (f32[16,4]{0,1:T(4,128)}, f32[16,4]{0,1:T(4,128)S(1)}, u32[]{:S(2)}) copy-start(f32[16,4]{0,1:T(4,128)S(1)} %copy.65) | copy-start | bytes 772
  170.8 4.9 %copy-start.3 = (bf16[16,4,128,128]{3,2,1,0:T(8,128)(2,1)S(1)}, bf16[16,4,128,128]{3,2,1,0:T(8,128)(2,1)}, u32[]{:S(2)}) copy-start(bf16[16,4,128,128]{3,2,1,0:T(8,128)(2,1)} %param.35) | copy-start | bytes 6291460
  175.7 2.3 copy-start.15
  175.7 2.3 copy-start.18
  175.8 24.9 %copy-start.6 = (bf16[512,512]{1,0:T(8,128)(2,1)S(1)}, bf16[512,512]{1,0:T(8,128)(2,1)}, u32[]{:S(2)}) copy-start(bf16[512,512]{1,0:T(8,128)(2,1)} %param.41) | copy-start | bytes 1572868
  184.2 2.3 copy-start.8
  184.2 2.3 copy-start.9
  184.2 2.3 copy-start.11
  184.2 2.3 copy-start.12
  184.2 2.3 copy-start.13
  184.2 2.3 copy-start.30
  201.6 119.3 %all-reduce.7.cloned.1.call-start = ((), (), s32[]{:S(2)}) async-start(), calls=%async_computation.11 | async-start | bytes 5767168 | tf_op jit(solution)/shard_map/psum | solution.py:164
  244.1 2.3 copy-start.2
  320.9 17.0 %copy-start.4 = (f32[128,512]{1,0:T(8,128)S(1)}, f32[128,512]{1,0:T(8,128)}, u32[]{:S(2)}) copy-start(f32[128,512]{1,0:T(8,128)} %all-reduce.5.cloned.1.call-done) | copy-start | bytes 786436
  324.4 7.1 %collective-permute-start = (f32[128,512]{1,0:T(8,128)S(1)}, f32[128,512]{1,0:T(8,128)S(1)}, u32[]{:S(2)}, u32[]{:S(2)}) collective-permute-start(f32[128,512]{1,0:T(8,128)S(1)} %fusion.2), channel_id=1, source_target_pairs={{0,8},{8,0},{16,24},{24,16},{1,9},{9,1},{17,25},{25,17},{2,10},{10... | collective-permute-start | bytes 786440 | tf_op jit(solution)/shard_map/ppermute | solution.py:169
  331.5 6.4 %collective-permute-start.1 = (f32[128,512]{1,0:T(8,128)S(1)}, f32[128,512]{1,0:T(8,128)S(1)}, u32[]{:S(2)}, u32[]{:S(2)}) collective-permute-start(f32[128,512]{1,0:T(8,128)S(1)} %add.145), channel_id=1, source_target_pairs={{0,16},{8,24},{16,0},{24,8},{1,17},{9,25},{17,1},{25,9},{2,18},{10... | collective-permute-start | bytes 786440 | tf_op jit(solution)/shard_map/ppermute | solution.py:169
  (10 other events, 22.4 us)
Sparse Core Ops, SparseCore 0:
  9.6 33.3 reduce-scatter.15
  45.2 28.5 reduce-scatter.17
  76.0 28.8 reduce-scatter.9
  107.0 28.8 reduce-scatter.11
  138.0 28.9 reduce-scatter.13
  201.7 41.2 all-reduce.4
  248.2 72.6 all-reduce.6
